TPU v7x, 32 devices: a whole 2x2x4 slice. The times are simulated.
32 devices in a mesh: sp: 8 (over z, y), tp: 4 (over x, core).
Axes of the slice: x: 2, y: 2, z: 4, core: 2. Of those that a mesh axis runs over, the one named last changes fastest.
Arguments:
- stream: bfloat16 [2048, 2048], P(('sp', 'tp')), may hold values from -6 to 6
- queries: bfloat16 [2048, 2048], P('sp', 'tp'), may hold values from -147.07821 to 147.07821
- keys: bfloat16 [2048, 2048], P('sp', 'tp'), may hold values from -7 to 7
- values: bfloat16 [2048, 2048], P('sp', 'tp'), may hold values from -6 to 6
- head_lambda: float32 [8], P('tp'), may hold values from 0.3 to 0.8
- head_gain: float32 [256], replicated, may hold values from 0.1 to 1.9
- w_out: bfloat16 [2048, 2048], P('tp'), may hold values from -0.125 to 0.125
- norm_gain: float32 [2048], replicated, may hold values from 0.1 to 1.9
- w_gate: bfloat16 [2048, 5632], P('sp', 'tp'), may hold values from -0.125 to 0.125
- w_up: bfloat16 [2048, 5632], P('sp', 'tp'), may hold values from -0.125 to 0.125
- w_down: bfloat16 [5632, 2048], P('tp', 'sp'), may hold values from -0.078125 to 0.078125
Outputs:
- result: bfloat16 [2048, 2048], P(('sp', 'tp'))
All inputs are finite; a program needn't handle non-finite values.
Results may differ from a plain program's by a relative error of at most 0.013.
Values may be sent and summed in bfloat16 or wider, within the bound.
A program may use at most 192 MiB of HBM per device.

v0:
```python
import jax
import jax.numpy as jnp
from jax import lax
from jax.sharding import PartitionSpec as P

epsilon = 1e-06


def normalize(values_in, gain):
    square_mean = jnp.mean(values_in * values_in, axis=-1, keepdims=True)
    return values_in * lax.rsqrt(square_mean + epsilon) * gain


def shards(
    stream, queries, keys, values, head_lambda, head_gain, w_out, norm_gain, w_gate, w_up, w_down
):
    row_count = queries.shape[0]
    head_count = head_lambda.shape[0]
    head_dim = queries.shape[1] // (2 * head_count)
    value_dim = values.shape[1] // head_count
    score_scale = head_dim ** (-0.5)
    offset = lax.axis_index("sp") * row_count
    query_heads = queries.reshape(row_count, head_count, 2, head_dim)
    query_pos = offset + jnp.arange(row_count, dtype=jnp.int32)
    start_state = (
        jnp.full((head_count, 2, row_count), -1e30, jnp.float32),
        jnp.zeros((head_count, 2, row_count), jnp.float32),
        jnp.zeros((head_count, 2, row_count, value_dim), jnp.float32),
    )
    key_piece = lax.all_gather(keys, "sp", axis=0, tiled=True)
    value_piece = lax.all_gather(values, "sp", axis=0, tiled=True)
    span = key_piece.shape[0]

    def update(state):
        row_max, weight_sum, partial_value = state
        key_heads = key_piece.reshape(span, head_count, 2, head_dim)
        value_heads = value_piece.reshape(span, head_count, value_dim)
        scores = (
            jnp.einsum(
                "qhsd,khsd->hsqk", query_heads, key_heads, preferred_element_type=jnp.float32
            )
            * score_scale
        )
        key_pos = jnp.arange(span, dtype=jnp.int32)
        visible = key_pos[None, :] <= query_pos[:, None]
        new_max = jnp.maximum(row_max, jnp.max(jnp.where(visible, scores, -1e30), axis=-1))
        weights = jnp.where(visible, jnp.exp(scores - new_max[..., None]), 0.0)
        new_sum = jnp.sum(weights, axis=-1)
        added = jnp.einsum(
            "hsqk,khd->hsqd",
            weights.astype(jnp.bfloat16),
            value_heads,
            preferred_element_type=jnp.float32,
        )
        return (new_max, new_sum, added)

    def unchanged(state):
        return state

    row_max, weight_sum, partial_value = lax.cond(
        jnp.int32(0) <= offset + row_count - 1, update, unchanged, start_state
    )
    map_out = partial_value / weight_sum[..., None]
    contrast = map_out[:, 0] - head_lambda[:, None, None] * map_out[:, 1]
    head_out = (
        normalize(contrast, head_gain)
        .transpose(1, 0, 2)
        .reshape(row_count, head_count * value_dim)
        .astype(jnp.bfloat16)
    )
    local_rows = stream.shape[0]
    projected = lax.psum(
        jnp.dot(head_out, w_out, preferred_element_type=jnp.float32).astype(jnp.bfloat16), "tp"
    ).astype(jnp.float32)
    stream_all = lax.all_gather(stream, "tp", axis=0, tiled=True)
    middle_all = stream_all.astype(jnp.float32) + projected
    mixer_in = normalize(middle_all, norm_gain).astype(jnp.bfloat16)
    middle = lax.dynamic_slice_in_dim(middle_all, lax.axis_index("tp") * local_rows, local_rows, 0)
    gate = jnp.dot(
        mixer_in,
        lax.all_gather(w_gate, "sp", axis=0, tiled=True),
        preferred_element_type=jnp.float32,
    )
    up_part = jnp.dot(
        mixer_in, lax.all_gather(w_up, "sp", axis=0, tiled=True), preferred_element_type=jnp.float32
    )
    down_full = lax.all_gather(w_down, "sp", axis=1, tiled=True)
    hidden = (jax.nn.silu(gate) * up_part).astype(jnp.bfloat16)
    mixed = lax.psum_scatter(
        jnp.dot(hidden, down_full, preferred_element_type=jnp.float32).astype(jnp.bfloat16),
        "tp",
        scatter_dimension=0,
        tiled=True,
    ).astype(jnp.float32)
    return (middle + mixed).astype(jnp.bfloat16)


def solution(mesh):
    placed = (
        P(("sp", "tp"), None),
        P("sp", "tp"),
        P("sp", "tp"),
        P("sp", "tp"),
        P("tp"),
        P(),
        P("tp", None),
        P(),
        P("sp", "tp"),
        P("sp", "tp"),
        P("tp", "sp"),
    )
    return jax.shard_map(
        shards, mesh=mesh, in_specs=placed, out_specs=P(("sp", "tp"), None), check_vma=False
    )
```

profile of v0, /device:TPU:0, one launch (start us, length us, event | category | flops | bytes accessed | tf_op | source)
XLA Modules:
  0.0 499.6 jit_solution(3734772541105203988)
XLA Ops:
  6.5 0.7 all-gather.11.cloned.1.call-update
  7.3 0.7 all-gather.9.cloned.1.call-update
  8.1 0.7 all-gather.7.cloned.1.call-update
  8.8 52.5 %all-gather.11.cloned.1.call-done = bf16[2048,512]{1,0:T(8,128)(2,1)} async-done(((bf16[256,512]{1,0:T(8,128)(2,1)}), bf16[2048,512]{1,0:T(8,128)(2,1)}) %all-gather.11.cloned.1.call-update) | async-done | bytes 2097168 | tf_op jit(solution)/shard_map/all_gather | solution.py:31
  61.3 49.8 %all-gather.9.cloned.1.call-done = bf16[2048,512]{1,0:T(8,128)(2,1)} async-done(((bf16[256,512]{1,0:T(8,128)(2,1)}), bf16[2048,512]{1,0:T(8,128)(2,1)}) %all-gather.9.cloned.1.call-update) | async-done | bytes 2097168 | tf_op jit(solution)/shard_map/all_gather | solution.py:30
  111.1 28.6 %conditional.1 = (f32[2,2,256]{2,1,0:T(2,128)S(1)}, f32[2,2,256,256]{2,3,0,1:T(8,128)S(1)}) conditional(s32[]{:T(128)} %convert_element_type.40, () %tuple.13, (s32[]{:T(128)}, s32[256]{0:T(256)S(1)}, bf16[256,512]{1,0:T(8,128)(2,1)}, bf16[2048,512]{1,0:T(8,128)(2,1)}, bf16[2048,512]{1,0:T(8,128)(2,1)}) %tuple.14), branch_computations={%region_0.0_spmd, %region_1.4_spmd} | conditional | flops 1634204928 | bytes 46951500 | solution.py:60
  111.5 4.2 reshape.34
  115.8 6.8 %select_reduce_fusion = (f32[2,2,256]{2,1,0:T(2,128)S(1)}, f32[2,2,256,2048]{3,2,1,0:T(8,128)}) fusion(pred[256,2048]{1,0:T(8,128)(4,1)S(1)} %iota_compare_fusion, bf16[2048,2,2,128]{3,2,1,0:T(2,128)(2,1)} %reshape.34, bf16[256,2,2,128]{3,2,1,0:T(2,128)(2,1)S(1)} %reshape.33), kind=kOutput, calls=%fused_computation.1 | convolution fusion | flops 543161344 | bytes 11276288 | tf_op jit(solution)/shard_map/cond/branch_1_fun/qhsd,khsd->hsqk/dot_general | solution.py:39
  122.6 4.0 reshape.35
  126.6 6.8 %fusion.2 = f32[2,2,256,256]{3,2,1,0:T(8,128)} fusion(f32[2,2,256,2048]{3,2,1,0:T(8,128)} %get-tuple-element.31, f32[2,2,256]{2,1,0:T(2,128)S(1)} %broadcast_maximum_fusion, pred[256,2048]{1,0:T(8,128)(4,1)S(1)} %iota_compare_fusion, bf16[2048,2,256,1]{2,1,0,3:T(2,128)(2,1)} %bitcast.27), kind=kOutput, calls=%fused_computation.4 | convolution fusion | flops 1082130432 | bytes 12062720 | tf_op jit(solution)/shard_map/cond/branch_1_fun/hsqk,khd->hsqd/dot_general | solution.py:49
  133.4 1.6 copy.26
  134.9 4.7 fusion.1
  140.6 1.7 convolution_convert_fusion
  142.4 0.5 all-gather.13.cloned.1.call-update
  143.6 0.7 all-gather.17.cloned.1.call-update
  144.6 32.8 %all-reduce.2.cloned.1.call-done = bf16[256,2048]{1,0:T(8,128)(2,1)} async-done(((bf16[256,2048]{1,0:T(8,128)(2,1)}), bf16[256,2048]{1,0:T(8,128)(2,1)}) %all-reduce.2.cloned.1.call-update) | async-done | bytes 1048592 | tf_op jit(solution)/shard_map/psum | solution.py:72
  177.3 3.2 convert_add_fusion
  180.6 91.6 %all-gather.13.cloned.1.call-done = bf16[2048,1408]{1,0:T(8,128)(2,1)} async-done(((bf16[256,1408]{1,0:T(8,128)(2,1)}), bf16[2048,1408]{1,0:T(8,128)(2,1)}) %all-gather.13.cloned.1.call-update) | async-done | bytes 5767184 | tf_op jit(solution)/shard_map/all_gather | solution.py:81
  272.2 5.9 %fusion.18 = f32[256,1408]{1,0:T(8,128)} fusion(bf16[2048,1408]{1,0:T(8,128)(2,1)} %all-gather.13.cloned.1.call-done, f32[2048]{0:T(1024)S(1)} %copy-done.6, f32[256]{0:T(256)S(1)} %add_rsqrt_fusion.1, bf16[256,2048]{1,0:T(8,128)(2,1)} %all-reduce.2.cloned.1.call-done, bf16[256,2048]{1,0:T(8,128)(2,1)S(1)} %copy-done.2), kind=kOutput, calls=%fused_computation.36 | convolution fusion | flops 1479540736 | bytes 9315328 | tf_op jit(solution)/shard_map/dot_general | solution.py:79
  278.1 86.6 %all-gather.15.cloned.1.call-done = bf16[2048,1408]{1,0:T(8,128)(2,1)} async-done(((bf16[256,1408]{1,0:T(8,128)(2,1)}), bf16[2048,1408]{1,0:T(8,128)(2,1)}) %all-gather.15.cloned.1.call-update) | async-done | bytes 5767184 | tf_op jit(solution)/shard_map/all_gather | solution.py:85
  364.8 93.4 %all-gather.17.cloned.1.call-done = bf16[1408,2048]{1,0:T(8,128)(2,1)} async-done(((bf16[1408,256]{1,0:T(8,128)(2,1)}), bf16[1408,2048]{1,0:T(8,128)(2,1)}) %all-gather.17.cloned.1.call-update) | async-done | bytes 5767184 | tf_op jit(solution)/shard_map/all_gather | solution.py:87
  458.1 9.6 %convolution_convert_fusion.1 = bf16[256,2048]{1,0:T(8,128)(2,1)} fusion(bf16[1408,2048]{1,0:T(8,128)(2,1)} %all-gather.17.cloned.1.call-done, bf16[2048,1408]{1,0:T(8,128)(2,1)} %all-gather.15.cloned.1.call-done, f32[256,1408]{1,0:T(8,128)} %fusion.18, f32[2048]{0:T(1024)S(1)} %copy-done.6, f32[256]{0:T(256)S(1)} %add_rsqrt_fusion.1, ...), kind=kOutput, calls=%fused_computation.21 | convolution fusion | flops 2958622720 | bytes 16131072 | tf_op jit(solution)/shard_map/dot_general | solution.py:90
  467.8 23.1 %reduce-scatter.2.cloned.1.call-done = bf16[64,2048]{1,0:T(8,128)(2,1)} async-done(((bf16[256,2048]{1,0:T(8,128)(2,1)}), bf16[64,2048]{1,0:T(8,128)(2,1)}) %reduce-scatter.2.cloned.1.call-update) | async-done | bytes 262160 | tf_op jit(solution)/shard_map/reduce_scatter | solution.py:89
  490.9 1.9 add_convert_fusion
  (37 shorter events, 2.4 us)
Async XLA Ops:
  6.5 134.1 %copy-start = (bf16[512,2048]{1,0:T(8,128)(2,1)S(1)}, bf16[512,2048]{1,0:T(8,128)(2,1)}, u32[]{:S(2)}) copy-start(bf16[512,2048]{1,0:T(8,128)(2,1)} %param.19) | copy-start | bytes 6291460
  6.5 54.8 %all-gather.11.cloned.1.call-start = ((), (), s32[]{:S(2)}) async-start(), calls=%async_computation.3 | async-start | bytes 2359296 | tf_op jit(solution)/shard_map/all_gather | solution.py:31
  7.3 103.8 %all-gather.9.cloned.1.call-start = ((), (), s32[]{:S(2)}) async-start(), calls=%async_computation.2 | async-start | bytes 2359296 | tf_op jit(solution)/shard_map/all_gather | solution.py:30
  8.0 136.6 %all-gather.7.cloned.1.call-start = ((), (), s32[]{:S(2)}) async-start(), calls=%async_computation.1 | async-start | bytes 1310720 | tf_op jit(solution)/shard_map/all_gather | solution.py:75
  8.7 168.6 %all-reduce.2.cloned.1.call-start = ((), (), s32[]{:S(2)}) async-start(), calls=%async_computation.4 | async-start | bytes 2097152 | tf_op jit(solution)/shard_map/psum | solution.py:72
  111.5 15.2 %copy-start.1 = (pred[256,2048]{1,0:T(8,128)(4,1)}, pred[256,2048]{1,0:T(8,128)(4,1)S(1)}, u32[]{:S(2)}) copy-start(pred[256,2048]{1,0:T(8,128)(4,1)S(1)} %iota_compare_fusion) | copy-start | bytes 1572868 | tf_op jit(solution)/shard_map/cond
  111.5 4.2 copy-start.3
  139.6 0.7 copy-start.4
  139.7 0.8 copy-start.5
  142.4 129.8 %all-gather.13.cloned.1.call-start = ((), (), s32[]{:S(2)}) async-start(), calls=%async_computation.5 | async-start | bytes 6488064 | tf_op jit(solution)/shard_map/all_gather | solution.py:81
  143.0 221.8 %all-gather.15.cloned.1.call-start = ((), (), s32[]{:S(2)}) async-start(), calls=%async_computation.6 | async-start | bytes 6488064 | tf_op jit(solution)/shard_map/all_gather | solution.py:85
  143.6 314.6 %all-gather.17.cloned.1.call-start = ((), (), s32[]{:S(2)}) async-start(), calls=%async_computation.7 | async-start | bytes 6488064 | tf_op jit(solution)/shard_map/all_gather | solution.py:87
  144.3 127.9 %copy-start.6 = (f32[2048]{0:T(1024)S(1)}, f32[2048]{0:T(1024)}, u32[]{:S(2)}) copy-start(f32[2048]{0:T(1024)} %param.20) | copy-start | bytes 24580
  144.3 346.6 %reduce-scatter.2.cloned.1.call-start = ((), (), s32[]{:S(2)}) async-start(), calls=%async_computation.8 | async-start | bytes 1310720 | tf_op jit(solution)/shard_map/reduce_scatter | solution.py:89
  144.6 127.6 %copy-start.2 = (bf16[256,2048]{1,0:T(8,128)(2,1)S(1)}, bf16[256,2048]{1,0:T(8,128)(2,1)}, u32[]{:S(2)}) copy-start(bf16[256,2048]{1,0:T(8,128)(2,1)} %all-gather.7.cloned.1.call-done) | copy-start | bytes 3145732
Sparse Core Ops, SparseCore 0:
  9.5 51.7 all-gather.10
  63.4 47.6 all-gather.8
  112.6 15.2 all-gather.6
  142.5 34.7 all-reduce.1
  179.4 92.7 all-gather.12
  274.2 90.4 all-gather.14
  366.8 91.2 all-gather.16
  467.9 22.9 reduce-scatter.1
where the time goes:
time: 500 us
  waiting for transfers between devices  434 us (87%)
  matrix products  30.9 us (6%)
  between operations  13.6 us (3%)
  other arithmetic  10.6 us (2%)
  local copies, waits for them, and re-layouts  10.4 us (2%)
    all_gather x1, waiting for transfers between devices, shards(): down_full = lax.all_gather(w_down, 'sp', axis=1, tiled=True)  93.4 us
    all_gather x1, waiting for transfers between devices, shards(): lax.all_gather(w_gate, 'sp', axis=0, tiled=True)  91.6 us
    all_gather x1, waiting for transfers between devices, shards(): lax.all_gather(w_up, 'sp', axis=0, tiled=True)  86.6 us
    all_gather x1, waiting for transfers between devices, shards(): value_piece = lax.all_gather(values, 'sp', axis=0, tiled=True)  52.5 us
    all_gather x1, waiting for transfers between devices, shards(): key_piece = lax.all_gather(keys, 'sp', axis=0, tiled=True)  49.8 us
    psum x1, waiting for transfers between devices, shards(): lax.psum(jnp.dot(head_out, w_out, preferred_element_type=jnp.float32).ast...  32.8 us
    reduce_scatter x1, waiting for transfers between devices, shards(): lax.psum_scatter(jnp.dot(hidden, down_full, preferred_element_type=jnp.fl...  23.1 us
  transfers between devices with their start and end apart: 8, of which 7 were waited for; matrix products, arithmetic and copies ran while one was open for 8% of the time, Pallas kernels for 0%

commit v1 on v0

--- a/solution.py
+++ b/solution.py
@@ -69,8 +69,11 @@
         .astype(jnp.bfloat16)
     )
     local_rows = stream.shape[0]
-    projected = lax.psum(
-        jnp.dot(head_out, w_out, preferred_element_type=jnp.float32).astype(jnp.bfloat16), "tp"
+    projected = jnp.sum(
+        lax.all_gather(
+            jnp.dot(head_out, w_out, preferred_element_type=jnp.float32).astype(jnp.bfloat16), "tp"
+        ),
+        axis=0,
     ).astype(jnp.float32)
     stream_all = lax.all_gather(stream, "tp", axis=0, tiled=True)
     middle_all = stream_all.astype(jnp.float32) + projected

time: 500 us -> 516 us (1.032)
  waiting for transfers between devices: 434 us -> 447 us
    psum x1 -> x0, waiting for transfers between devices: 32.8 us -> none  [shards(): lax.psum(jnp.dot(head_out, w_out, preferred_element_type=jnp.float32).ast...]
    all_gather x0 -> x1, waiting for transfers between devices: none -> 30.4 us  [shards(): lax.all_gather(jnp.dot(head_out, w_out, preferred_element_type=jnp.float3...]
    all_gather x1, waiting for transfers between devices: 0.02 us -> 15.1 us  [shards(): stream_all = lax.all_gather(stream, 'tp', axis=0, tiled=True)]
  transfers between devices with their start and end apart: 8 -> 8, of which waited for: 7 -> 8; matrix products, arithmetic and copies ran while one was open for 8% -> 2% of each run, Pallas kernels for 0% -> 0%
where the time goes in v1:
time: 516 us; the launch traced here: 515 us
  waiting for transfers between devices  447 us (87%)
  matrix products  30.8 us (6%)
  between operations  13.6 us (3%)
  other arithmetic  13.3 us (3%)
  local copies, waits for them, and re-layouts  10.4 us (2%)
    all_gather x1, waiting for transfers between devices, shards(): down_full = lax.all_gather(w_down, 'sp', axis=1, tiled=True)  93.4 us
    all_gather x1, waiting for transfers between devices, shards(): lax.all_gather(w_gate, 'sp', axis=0, tiled=True)  91.5 us
    all_gather x1, waiting for transfers between devices, shards(): lax.all_gather(w_up, 'sp', axis=0, tiled=True)  86.6 us
    all_gather x1, waiting for transfers between devices, shards(): key_piece = lax.all_gather(keys, 'sp', axis=0, tiled=True)  53.2 us
    all_gather x1, waiting for transfers between devices, shards(): value_piece = lax.all_gather(values, 'sp', axis=0, tiled=True)  49.8 us
    all_gather x1, waiting for transfers between devices, shards(): lax.all_gather(jnp.dot(head_out, w_out, preferred_element_type=jnp.float3...  30.4 us
    reduce_scatter x1, waiting for transfers between devices, shards(): lax.psum_scatter(jnp.dot(hidden, down_full, preferred_element_type=jnp.fl...  23.1 us
    all_gather x1, waiting for transfers between devices, shards(): stream_all = lax.all_gather(stream, 'tp', axis=0, tiled=True)  15.1 us
  transfers between devices with their start and end apart: 8, of which 8 were waited for; matrix products, arithmetic and copies ran while one was open for 2% of the time, Pallas kernels for 0%

profile of v1, /device:TPU:0, one launch (start us, length us, event | category | flops | bytes accessed | tf_op | source)
XLA Modules:
  0.0 515.4 jit_solution(10457912026612638012)
XLA Ops:
  6.5 0.7 all-gather.11.cloned.1.call-update
  7.3 0.7 all-gather.13.cloned.1.call-update
  8.1 53.2 %all-gather.11.cloned.1.call-done = bf16[2048,512]{1,0:T(8,128)(2,1)} async-done(((bf16[256,512]{1,0:T(8,128)(2,1)}), bf16[2048,512]{1,0:T(8,128)(2,1)}) %all-gather.11.cloned.1.call-update) | async-done | bytes 2097168 | tf_op jit(solution)/shard_map/all_gather | solution.py:30
  61.3 49.8 %all-gather.13.cloned.1.call-done = bf16[2048,512]{1,0:T(8,128)(2,1)} async-done(((bf16[256,512]{1,0:T(8,128)(2,1)}), bf16[2048,512]{1,0:T(8,128)(2,1)}) %all-gather.13.cloned.1.call-update) | async-done | bytes 2097168 | tf_op jit(solution)/shard_map/all_gather | solution.py:31
  111.1 28.5 %conditional.1 = (f32[2,2,256]{2,1,0:T(2,128)S(1)}, f32[2,2,256,256]{2,3,0,1:T(8,128)S(1)}) conditional(s32[]{:T(128)} %convert_element_type.42, () %tuple.13, (s32[]{:T(128)}, s32[256]{0:T(256)S(1)}, bf16[256,512]{1,0:T(8,128)(2,1)}, bf16[2048,512]{1,0:T(8,128)(2,1)}, bf16[2048,512]{1,0:T(8,128)(2,1)}) %tuple.14), branch_computations={%region_0.0_spmd, %region_1.4_spmd} | conditional | flops 1634204928 | bytes 46951500 | solution.py:60
  111.5 4.2 reshape.34
  115.7 6.8 %select_reduce_fusion = (f32[2,2,256]{2,1,0:T(2,128)S(1)}, f32[2,2,256,2048]{3,2,1,0:T(8,128)}) fusion(pred[256,2048]{1,0:T(8,128)(4,1)S(1)} %iota_compare_fusion, bf16[2048,2,2,128]{3,2,1,0:T(2,128)(2,1)} %reshape.34, bf16[256,2,2,128]{3,2,1,0:T(2,128)(2,1)S(1)} %reshape.33), kind=kOutput, calls=%fused_computation.1 | convolution fusion | flops 543161344 | bytes 11276288 | tf_op jit(solution)/shard_map/cond/branch_1_fun/qhsd,khsd->hsqk/dot_general | solution.py:39
  122.6 4.0 reshape.35
  126.6 6.7 %fusion.2 = f32[2,2,256,256]{3,2,1,0:T(8,128)} fusion(f32[2,2,256,2048]{3,2,1,0:T(8,128)} %get-tuple-element.31, f32[2,2,256]{2,1,0:T(2,128)S(1)} %broadcast_maximum_fusion, pred[256,2048]{1,0:T(8,128)(4,1)S(1)} %iota_compare_fusion, bf16[2048,2,256,1]{2,1,0,3:T(2,128)(2,1)} %bitcast.29), kind=kOutput, calls=%fused_computation.4 | convolution fusion | flops 1082130432 | bytes 12062720 | tf_op jit(solution)/shard_map/cond/branch_1_fun/hsqk,khd->hsqd/dot_general | solution.py:49
  133.3 1.6 copy.26
  134.9 4.7 fusion.1
  140.6 1.7 convolution_convert_fusion
  144.1 0.7 all-gather.19.cloned.1.call-update
  145.0 30.4 %all-gather.21.cloned.1.call-done = bf16[1024,2048]{1,0:T(8,128)(2,1)} async-done(((bf16[256,2048]{1,0:T(8,128)(2,1)}), bf16[1024,2048]{1,0:T(8,128)(2,1)}) %all-gather.21.cloned.1.call-update) | async-done | bytes 4194320 | tf_op jit(solution)/shard_map/all_gather | solution.py:73
  175.4 3.1 reduce_sum.40
  178.5 15.1 %all-gather.9.cloned.1.call-done = bf16[256,2048]{1,0:T(8,128)(2,1)} async-done(((bf16[64,2048]{1,0:T(8,128)(2,1)}), bf16[256,2048]{1,0:T(8,128)(2,1)}) %all-gather.9.cloned.1.call-update) | async-done | bytes 1048592 | tf_op jit(solution)/shard_map/all_gather | solution.py:78
  193.6 2.9 convert_add_fusion
  196.5 91.5 %all-gather.15.cloned.1.call-done = bf16[2048,1408]{1,0:T(8,128)(2,1)} async-done(((bf16[256,1408]{1,0:T(8,128)(2,1)}), bf16[2048,1408]{1,0:T(8,128)(2,1)}) %all-gather.15.cloned.1.call-update) | async-done | bytes 5767184 | tf_op jit(solution)/shard_map/all_gather | solution.py:84
  288.0 5.9 %fusion.18 = f32[256,1408]{1,0:T(8,128)} fusion(bf16[2048,1408]{1,0:T(8,128)(2,1)} %all-gather.15.cloned.1.call-done, f32[2048]{0:T(1024)S(1)} %copy-done.5, f32[256]{0:T(256)S(1)} %add_rsqrt_fusion.1, bf16[256,2048]{1,0:T(8,128)(2,1)S(1)} %reduce_sum.40, bf16[256,2048]{1,0:T(8,128)(2,1)} %all-gather.9.cloned.1.call-done), kind=kOutput, calls=%fused_computation.36 | convolution fusion | flops 1479540736 | bytes 9315328 | tf_op jit(solution)/shard_map/dot_general | solution.py:82
  293.9 86.6 %all-gather.17.cloned.1.call-done = bf16[2048,1408]{1,0:T(8,128)(2,1)} async-done(((bf16[256,1408]{1,0:T(8,128)(2,1)}), bf16[2048,1408]{1,0:T(8,128)(2,1)}) %all-gather.17.cloned.1.call-update) | async-done | bytes 5767184 | tf_op jit(solution)/shard_map/all_gather | solution.py:88
  380.5 93.4 %all-gather.19.cloned.1.call-done = bf16[1408,2048]{1,0:T(8,128)(2,1)} async-done(((bf16[1408,256]{1,0:T(8,128)(2,1)}), bf16[1408,2048]{1,0:T(8,128)(2,1)}) %all-gather.19.cloned.1.call-update) | async-done | bytes 5767184 | tf_op jit(solution)/shard_map/all_gather | solution.py:90
  473.9 9.7 %convolution_convert_fusion.1 = bf16[256,2048]{1,0:T(8,128)(2,1)} fusion(bf16[1408,2048]{1,0:T(8,128)(2,1)} %all-gather.19.cloned.1.call-done, bf16[2048,1408]{1,0:T(8,128)(2,1)} %all-gather.17.cloned.1.call-done, f32[256,1408]{1,0:T(8,128)} %fusion.18, f32[2048]{0:T(1024)S(1)} %copy-done.5, f32[256]{0:T(256)S(1)} %add_rsqrt_fusion.1, ...), kind=kOutput, calls=%fused_computation.21 | convolution fusion | flops 2958622720 | bytes 16131072 | tf_op jit(solution)/shard_map/dot_general | solution.py:93
  483.6 23.1 %reduce-scatter.2.cloned.1.call-done = bf16[64,2048]{1,0:T(8,128)(2,1)} async-done(((bf16[256,2048]{1,0:T(8,128)(2,1)}), bf16[64,2048]{1,0:T(8,128)(2,1)}) %reduce-scatter.2.cloned.1.call-update) | async-done | bytes 262160 | tf_op jit(solution)/shard_map/reduce_scatter | solution.py:92
  506.7 1.9 add_convert_fusion
  (36 shorter events, 3.5 us)
Async XLA Ops:
  6.5 134.0 %copy-start = (bf16[512,2048]{1,0:T(8,128)(2,1)S(1)}, bf16[512,2048]{1,0:T(8,128)(2,1)}, u32[]{:S(2)}) copy-start(bf16[512,2048]{1,0:T(8,128)(2,1)} %param.19) | copy-start | bytes 6291460
  6.5 54.8 %all-gather.11.cloned.1.call-start = ((), (), s32[]{:S(2)}) async-start(), calls=%async_computation.2 | async-start | bytes 2359296 | tf_op jit(solution)/shard_map/all_gather | solution.py:30
  7.3 103.8 %all-gather.13.cloned.1.call-start = ((), (), s32[]{:S(2)}) async-start(), calls=%async_computation.3 | async-start | bytes 2359296 | tf_op jit(solution)/shard_map/all_gather | solution.py:31
  8.0 167.4 %all-gather.21.cloned.1.call-start = ((), (), s32[]{:S(2)}) async-start(), calls=%async_computation.8 | async-start | bytes 5242880 | tf_op jit(solution)/shard_map/all_gather | solution.py:73
  111.5 15.1 %copy-start.1 = (pred[256,2048]{1,0:T(8,128)(4,1)}, pred[256,2048]{1,0:T(8,128)(4,1)S(1)}, u32[]{:S(2)}) copy-start(pred[256,2048]{1,0:T(8,128)(4,1)S(1)} %iota_compare_fusion) | copy-start | bytes 1572868 | tf_op jit(solution)/shard_map/cond
  111.5 4.2 copy-start.2
  139.6 0.7 copy-start.3
  139.6 0.8 copy-start.4
  142.3 51.3 %all-gather.9.cloned.1.call-start = ((), (), s32[]{:S(2)}) async-start(), calls=%async_computation.1 | async-start | bytes 1310720 | tf_op jit(solution)/shard_map/all_gather | solution.py:78
  142.9 145.1 %all-gather.15.cloned.1.call-start = ((), (), s32[]{:S(2)}) async-start(), calls=%async_computation.4 | async-start | bytes 6488064 | tf_op jit(solution)/shard_map/all_gather | solution.py:84
  143.4 237.1 %all-gather.17.cloned.1.call-start = ((), (), s32[]{:S(2)}) async-start(), calls=%async_computation.5 | async-start | bytes 6488064 | tf_op jit(solution)/shard_map/all_gather | solution.py:88
  144.0 329.9 %all-gather.19.cloned.1.call-start = ((), (), s32[]{:S(2)}) async-start(), calls=%async_computation.6 | async-start | bytes 6488064 | tf_op jit(solution)/shard_map/all_gather | solution.py:90
  144.8 361.9 %reduce-scatter.2.cloned.1.call-start = ((), (), s32[]{:S(2)}) async-start(), calls=%async_computation.7 | async-start | bytes 1310720 | tf_op jit(solution)/shard_map/reduce_scatter | solution.py:92
  178.5 109.4 %copy-start.5 = (f32[2048]{0:T(1024)S(1)}, f32[2048]{0:T(1024)}, u32[]{:S(2)}) copy-start(f32[2048]{0:T(1024)} %param.20) | copy-start | bytes 24580
Sparse Core Ops, SparseCore 0:
  9.5 51.7 all-gather.10
  63.4 47.6 all-gather.12
  142.4 32.9 all-gather.20
  176.8 16.6 all-gather.8
  195.6 92.3 all-gather.14
  290.0 90.4 all-gather.16
  382.6 91.2 all-gather.18
  483.7 22.9 reduce-scatter.1
